TPU v7x, 32 devices: a whole 2x2x4 slice. The times are simulated.
32 devices in a mesh: grp: 2 (over y), sp: 4 (over z), tp: 4 (over x, core).
Axes of the slice: x: 2, y: 2, z: 4, core: 2. Of those that a mesh axis runs over, the one named last changes fastest.
Arguments:
- conv_input: bfloat16 [4096, 1024], P(('grp', 'sp'), 'tp'), parts along dimension 0, may hold values from -6 to 6
- pre_gate: bfloat16 [4096, 1024], P(('grp', 'sp'), 'tp'), parts along dimension 0, may hold values from -6 to 6
- post_gate: bfloat16 [4096, 1024], P(('grp', 'sp'), 'tp'), parts along dimension 0, may hold values from -6 to 6
- conv_taps: float32 [3, 1024], replicated, may hold values from -3.5 to 3.5
- out_proj: bfloat16 [1024, 2048], replicated, may hold values from -0.1875 to 0.1875
- residual_in: bfloat16 [4096, 2048], P(('grp', 'sp', 'tp')), parts along dimension 0, may hold values from -6 to 6
- norm_gain: float32 [2048], replicated, may hold values from 0.1 to 1.9
- routes: int32 [4096, 2], P(('grp', 'sp', 'tp')), parts along dimension 0, may hold values from 0 to 7, as said below
- route_weight: float32 [4096, 2], P(('grp', 'sp', 'tp')), parts along dimension 0, may hold values from 0.1 to 1
- w_gate: bfloat16 [8, 2048, 1024], P('sp', None, 'tp'), may hold values from -0.125 to 0.125
- w_up: bfloat16 [8, 2048, 1024], P('sp', None, 'tp'), may hold values from -0.125 to 0.125
- w_down: bfloat16 [8, 1024, 2048], P('sp', 'tp'), may hold values from -0.1875 to 0.1875
Outputs:
- layer_out: bfloat16 [4096, 2048], P(('grp', 'sp', 'tp')), parts along dimension 0
There are 2 independent parts, one for each index of `grp`. A program takes and returns all parts, laid end to end along the dimension named above; an argument that names none is the same for every part. Nothing has to cross between parts.
Inputs may be any that keep to these rules, and one draw needn't show every extreme that they name: `routes`: the two numbers of a row differ and lie in the same group of 2 consecutive experts. In each aligned block of 128 rows every expert is named exactly 32 times.
All inputs are finite; a program needn't handle non-finite values.
Results may differ from a plain program's by a relative error of at most 0.0085.
Values may be sent and summed in bfloat16 or wider, within the bound.
No kernel may reach another device: no remote copies, remote signals or barrier semaphores. Data moves between devices by JAX's collectives and lax.ppermute only.
A program may use at most 64 MiB of HBM per device.

v0:
```python
import jax
import jax.numpy as jnp
from jax import lax
from jax.sharding import PartitionSpec as P

GROUPS = 4
LANES = 128


def shifted(block, axis, distance):
    devices = range(lax.axis_size(axis))
    route = [(i - distance, i) for i in devices if i - distance in devices]
    return lax.ppermute(block, axis, route)


def flipped(block, axis, bit):
    return lax.ppermute(block, axis, [(i, i ^ bit) for i in range(lax.axis_size(axis))])


def mix(conv_input, pre_gate, post_gate, conv_taps):
    channels = conv_input.shape[1]
    taps = lax.dynamic_slice_in_dim(conv_taps, lax.axis_index("tp") * channels, channels, 1)
    edge = jnp.concatenate([conv_input[-2:], pre_gate[-2:]], axis=1)
    prior = shifted(edge, "sp", 1)
    prior_input, prior_gate = (prior[:, :channels], prior[:, channels:])
    gated = jnp.concatenate(
        [
            prior_gate.astype(jnp.float32) * prior_input.astype(jnp.float32),
            pre_gate.astype(jnp.float32) * conv_input.astype(jnp.float32),
        ],
        axis=0,
    )
    conv = gated[2:] * taps[2] + gated[1:-1] * taps[1] + gated[:-2] * taps[0]
    return (post_gate.astype(jnp.float32) * conv).astype(jnp.bfloat16)


def project(mixed, out_proj, residual_in, norm_gain):
    token_rows = lax.all_to_all(mixed, "tp", split_axis=0, concat_axis=1, tiled=True)
    projected = jnp.dot(token_rows, out_proj, preferred_element_type=jnp.float32)
    stream = residual_in.astype(jnp.float32) + projected
    scale = lax.rsqrt(jnp.mean(stream * stream, axis=-1, keepdims=True) + 1e-06)
    normed = (stream * scale * norm_gain).astype(jnp.bfloat16)
    return (stream, normed)


def route_by_group(stream, normed, routes, route_weight, w_gate, w_up, w_down):
    shards = lax.axis_size("tp")
    seq_ranks = lax.axis_size("sp")
    block_rows, width = stream.shape
    local_experts = w_gate.shape[0]
    capacity = block_rows // seq_ranks
    group = routes[:, 0] // local_experts
    order = jnp.arange(block_rows, dtype=jnp.int32)
    earlier = (group[:, None] == group[None, :]) & (order[None, :] < order[:, None])
    slot = group * capacity + jnp.sum(earlier.astype(jnp.int32), axis=1)
    select = (order[:, None] == slot[None, :]).astype(jnp.bfloat16)
    member = routes[:, :, None] % local_experts == jnp.arange(local_experts, dtype=jnp.int32)
    weight = jnp.sum(jnp.where(member, route_weight[:, :, None], 0.0), axis=1)
    high = lax.reduce_precision(weight, 8, 7)
    labels = jnp.concatenate([high, weight - high], axis=1).astype(jnp.bfloat16)
    labels = jnp.pad(labels, ((0, 0), (0, LANES - labels.shape[1])))
    rows = jnp.concatenate([normed, labels], axis=1)
    outgoing = jnp.dot(select, rows, preferred_element_type=jnp.float32).astype(jnp.bfloat16)
    outgoing = outgoing.reshape(seq_ranks, capacity, width + LANES)
    arrived = lax.all_to_all(outgoing, "sp", split_axis=0, concat_axis=0, tiled=True)
    blocks = {0: arrived.reshape(block_rows, width + LANES)}
    bits = [1 << b for b in range(shards.bit_length() - 1)]
    for bit in reversed(bits):
        blocks.update({k | bit: flipped(v, "tp", bit) for k, v in blocks.items()})
    down = w_down.reshape(local_experts * w_down.shape[1], width)
    parts = {}
    for k, block in blocks.items():
        features = block[:, :width]
        marks = block[:, width:].astype(jnp.float32)
        hidden = []
        for expert in range(local_experts):
            gate = jnp.dot(features, w_gate[expert], preferred_element_type=jnp.float32)
            upper = jnp.dot(features, w_up[expert], preferred_element_type=jnp.float32)
            scale = marks[:, expert] + marks[:, local_experts + expert]
            hidden.append((jax.nn.silu(gate) * upper * scale[:, None]).astype(jnp.bfloat16))
        hidden = jnp.concatenate(hidden, axis=1)
        parts[k] = jnp.dot(hidden, down, preferred_element_type=jnp.float32)
    for bit in bits:
        for k in [k for k in parts if k & bit]:
            parts[k ^ bit] += flipped(parts.pop(k).astype(jnp.bfloat16), "tp", bit).astype(
                jnp.float32
            )
    summed = parts[0].astype(jnp.bfloat16).reshape(seq_ranks, capacity, width)
    returned = lax.all_to_all(summed, "sp", split_axis=0, concat_axis=0, tiled=True)
    weighted = lax.dot_general(
        select,
        returned.reshape(block_rows, width),
        (((0,), (0,)), ((), ())),
        preferred_element_type=jnp.float32,
    )
    return (stream + weighted).astype(jnp.bfloat16)


def route_by_expert(stream, normed, routes, route_weight, w_gate, w_up, w_down):
    shards = lax.axis_size("tp")
    seq_ranks = lax.axis_size("sp")
    block_rows, width = stream.shape
    local_experts = w_gate.shape[0]
    experts = local_experts * seq_ranks
    capacity = 2 * block_rows // experts
    flat_routes = routes.reshape(-1)
    position = jnp.arange(flat_routes.shape[0], dtype=jnp.int32)
    earlier = (flat_routes[:, None] == flat_routes[None, :]) & (
        position[None, :] < position[:, None]
    )
    rank = jnp.sum(earlier.astype(jnp.int32), axis=1)
    slot = flat_routes * capacity + rank
    outgoing = (
        jnp.zeros((experts * capacity, width), jnp.bfloat16).at[slot].set(normed[position // 2])
    )
    outgoing = outgoing.reshape(seq_ranks, local_experts, capacity, width)
    spread = lax.all_gather(
        lax.all_to_all(outgoing, "sp", split_axis=0, concat_axis=0, tiled=True)[:, None],
        "tp",
        axis=1,
        tiled=True,
    )
    count = spread.shape[3]
    partials = []
    for expert in range(local_experts):
        rows = spread[:, :, expert].reshape(seq_ranks * shards * count, width)
        gate = jnp.dot(rows, w_gate[expert], preferred_element_type=jnp.float32)
        upper = jnp.dot(rows, w_up[expert], preferred_element_type=jnp.float32)
        hidden = (jax.nn.silu(gate) * upper).astype(jnp.bfloat16)
        part = jnp.dot(hidden, w_down[expert], preferred_element_type=jnp.float32).astype(
            jnp.bfloat16
        )
        partials.append(part.reshape(seq_ranks, shards, count, width))
    stacked = jnp.stack(partials, axis=2)
    summed = lax.psum_scatter(stacked, "tp", scatter_dimension=1, tiled=True).astype(jnp.float32)
    returned = lax.all_to_all(
        summed[:, 0].astype(jnp.bfloat16), "sp", split_axis=0, concat_axis=0, tiled=True
    )
    results = returned.reshape(experts * capacity, width)[slot]
    results = results.reshape(block_rows, 2, width).astype(jnp.float32)
    weighted = jnp.sum(route_weight[:, :, None] * results, axis=1)
    return (stream + weighted).astype(jnp.bfloat16)


def on_device(
    conv_input,
    pre_gate,
    post_gate,
    conv_taps,
    out_proj,
    residual_in,
    norm_gain,
    routes,
    route_weight,
    w_gate,
    w_up,
    w_down,
):
    shards = lax.axis_size("tp")
    mixed = mix(conv_input, pre_gate, post_gate, conv_taps)
    stream, normed = project(mixed, out_proj, residual_in, norm_gain)
    whole_groups = lax.axis_size("sp") == GROUPS and shards & shards - 1 == 0
    route = route_by_group if whole_groups else route_by_expert
    return route(stream, normed, routes, route_weight, w_gate, w_up, w_down)


def solution(mesh):
    return jax.shard_map(
        on_device,
        mesh=mesh,
        in_specs=(
            P(("grp", "sp"), "tp"),
            P(("grp", "sp"), "tp"),
            P(("grp", "sp"), "tp"),
            P(),
            P(),
            P(("grp", "sp", "tp"), None),
            P(),
            P(("grp", "sp", "tp"), None),
            P(("grp", "sp", "tp"), None),
            P("sp", None, "tp"),
            P("sp", None, "tp"),
            P("sp", "tp", None),
        ),
        out_specs=P(("grp", "sp", "tp"), None),
        check_vma=False,
    )
```

profile of v0, /device:TPU:0, one launch (start us, length us, event | category | flops | bytes accessed | tf_op | source)
XLA Modules:
  0.0 97.2 jit_solution(9595113881826151975)
XLA Ops:
  0.0 0.8 slice.127
  0.8 0.7 slice.128
  1.5 5.0 %collective-permute-start = (bf16[2,512]{1,0:T(2,128)(2,1)S(1)}, bf16[2,512]{1,0:T(2,128)(2,1)S(1)}, u32[]{:S(2)}, u32[]{:S(2)}) collective-permute-start(bf16[2,512]{1,0:T(2,128)(2,1)S(1)} %pad_maximum_fusion.1), channel_id=1, source_target_pairs={{0,4},{4,8},{8,12},{1,5},{5,9},{9,13},{2,6},{6,10},{10,14},{3,7},{... | collective-permute-start | bytes 6152 | tf_op jit(solution)/shard_map/ppermute | solution.py:13
  6.5 0.7 fusion.111
  7.2 0.7 and_select_fusion.2
  7.9 0.7 and_select_fusion
  8.6 1.1 %convert_multiply_fusion = f32[512,256]{1,0:T(8,128)S(1)} fusion(bf16[512,256]{1,0:T(8,128)(2,1)} %param.12, bf16[512,256]{1,0:T(8,128)(2,1)} %param.13), kind=kLoop, calls=%fused_computation.78 | loop fusion | flops 393216 | bytes 1048576 | tf_op jit(solution)/shard_map/mul | solution.py:29
  9.7 0.7 fusion.108
  10.6 0.9 fusion.119
  11.6 1.9 %fusion.62 = bf16[512,256]{1,0:T(8,128)(2,1)} fusion(f32[2,256]{1,0:T(2,128)S(1)} %convert_multiply_fusion.1, f32[512,256]{1,0:T(8,128)S(1)} %convert_multiply_fusion, bf16[512,256]{1,0:T(8,128)(2,1)} %param.14, f32[256]{0:T(256)S(1)} %bitcast.96, f32[256]{0:T(256)S(1)} %bitcast.95, f32[256]{0:T(256)S(1)} %bitcast.94), kind=kLoop, calls=%fused_computation.75 | loop fusion | flops 1310720 | bytes 1053696 | tf_op jit(solution)/shard_map/convert_element_type | solution.py:34
  13.5 3.4 %all-to-all-start = ((bf16[4,128,256]{2,1,0:T(8,128)(2,1)}), bf16[4,128,256]{2,1,0:T(8,128)(2,1)S(1)}, u32[]{:S(2)}, u32[]{:S(2)}) async-start(bf16[4,128,256]{2,1,0:T(8,128)(2,1)} %bitcast.3), calls=%async_computation | async-start | bytes 524288 | tf_op jit(solution)/shard_map/all_to_all | solution.py:38
  16.9 5.9 %all-to-all-done = bf16[4,128,256]{2,1,0:T(8,128)(2,1)S(1)} async-done(((bf16[4,128,256]{2,1,0:T(8,128)(2,1)}), bf16[4,128,256]{2,1,0:T(8,128)(2,1)S(1)}, u32[]{:S(2)}, u32[]{:S(2)}) %all-to-all-start) | async-done | bytes 262176 | tf_op jit(solution)/shard_map/all_to_all | solution.py:38
  23.0 3.0 %multiply_reduce_fusion = (f32[128]{0:T(128)S(1)}, f32[128,2048]{1,0:T(8,128)S(1)}) fusion(bf16[128,1024]{0,1:T(8,128)(2,1)S(1)} %bitcast.84, bf16[1024,2048]{1,0:T(8,128)(2,1)} %param.16, bf16[128,2048]{1,0:T(8,128)(2,1)S(1)} %copy-done.1), kind=kOutput, calls=%fused_computation.47 | convolution fusion | flops 537919360 | bytes 6029824 | tf_op jit(solution)/shard_map/dot_general | solution.py:39
  26.6 18.7 %all_to_all.29 = bf16[4,32,2176]{2,1,0:T(8,128)(2,1)S(1)} all-to-all(bf16[4,32,2176]{2,1,0:T(8,128)(2,1)S(1)} %bitcast.93), channel_id=1, replica_groups=mesh['grp'=2,'sp'=4,'tp'=4] {'sp'}, dimensions={0} | all-to-all | bytes 1114112 | tf_op jit(solution)/shard_map/all_to_all | solution.py:65
  45.3 0.8 collective-permute-start.3
  46.6 0.3 fusion.34
  47.0 0.3 fusion.4
  47.3 0.8 collective-permute-done.1
  48.2 0.3 fusion.17
  49.6 0.4 convolution_convert_fusion.2
  50.0 8.4 %collective-permute-done.3 = bf16[128,2176]{1,0:T(8,128)(2,1)S(1)} collective-permute-done((bf16[128,2176]{1,0:T(8,128)(2,1)S(1)}, bf16[128,2176]{1,0:T(8,128)(2,1)S(1)}, u32[]{:S(2)}, u32[]{:S(2)}) %collective-permute-start.3) | collective-permute-done | bytes 557088 | tf_op jit(solution)/shard_map/ppermute | solution.py:17
  58.6 0.6 collective-permute-start.2
  59.9 0.5 collective-permute-done.4
  61.3 0.3 multiply_convert_fusion.1
  61.9 0.4 convolution_convert_fusion.1
  63.2 1.1 %collective-permute-done.5 = bf16[128,2048]{1,0:T(8,128)(2,1)S(1)} collective-permute-done((bf16[128,2048]{1,0:T(8,128)(2,1)S(1)}, bf16[128,2048]{1,0:T(8,128)(2,1)S(1)}, u32[]{:S(2)}, u32[]{:S(2)}) %collective-permute-start.5) | collective-permute-done | bytes 524320 | tf_op jit(solution)/shard_map/ppermute | solution.py:17
  64.3 0.4 add_convert_fusion.1
  64.8 1.4 %collective-permute-start.6 = (bf16[128,2048]{1,0:T(8,128)(2,1)S(1)}, bf16[128,2048]{1,0:T(8,128)(2,1)S(1)}, u32[]{:S(2)}, u32[]{:S(2)}) collective-permute-start(bf16[128,2048]{1,0:T(8,128)(2,1)S(1)} %add_convert_fusion.1), channel_id=1, source_target_pairs={{0,2},{1,3},{2,0},{3,1},{4,6},{5,7},{6,4},{7,5},{8,10},{9,11},{10,... | collective-permute-start | bytes 1572872 | tf_op jit(solution)/shard_map/ppermute | solution.py:17
  66.5 0.4 fusion.81
  67.0 11.9 %collective-permute-done.6 = bf16[128,2048]{1,0:T(8,128)(2,1)S(1)} collective-permute-done((bf16[128,2048]{1,0:T(8,128)(2,1)S(1)}, bf16[128,2048]{1,0:T(8,128)(2,1)S(1)}, u32[]{:S(2)}, u32[]{:S(2)}) %collective-permute-start.6) | collective-permute-done | bytes 524320 | tf_op jit(solution)/shard_map/ppermute | solution.py:17
  79.0 17.0 %all_to_all.30 = bf16[4,32,2048]{2,1,0:T(8,128)(2,1)S(1)} all-to-all(bf16[4,32,2048]{2,1,0:T(8,128)(2,1)S(1)} %bitcast.82), channel_id=1, replica_groups=mesh['grp'=2,'sp'=4,'tp'=4] {'sp'}, dimensions={0} | all-to-all | bytes 1048576 | tf_op jit(solution)/shard_map/all_to_all | solution.py:89
  96.1 1.1 %fusion = bf16[128,2048]{1,0:T(8,128)(2,1)} fusion(f32[128,2048]{1,0:T(8,128)S(1)} %get-tuple-element.19, bf16[128,2048]{1,0:T(8,128)(2,1)S(1)} %bitcast.83, s32[128]{0:T(128)S(1)} %multiply_add_fusion), kind=kOutput, calls=%fused_computation.3 | convolution fusion | flops 67649536 | bytes 2097664 | tf_op jit(solution)/shard_map/dot_general | solution.py:90
  (49 shorter events, 6.1 us)
Async XLA Ops:
  0.0 49.6 %copy-start = (bf16[2,256,2048]{2,1,0:T(8,128)(2,1)S(1)}, bf16[2,256,2048]{2,1,0:T(8,128)(2,1)}, u32[]{:S(2)}) copy-start(bf16[2,256,2048]{2,1,0:T(8,128)(2,1)} %param.23) | copy-start | bytes 6291460
  0.0 16.9 %copy-start.3 = (s32[128,2]{0,1:T(2,128)S(1)}, s32[128,2]{0,1:T(2,128)}, u32[]{:S(2)}) copy-start(s32[128,2]{0,1:T(2,128)} %param.19) | copy-start | bytes 3076
  0.0 23.0 %copy-start.1 = (bf16[128,2048]{1,0:T(8,128)(2,1)S(1)}, bf16[128,2048]{1,0:T(8,128)(2,1)}, u32[]{:S(2)}) copy-start(bf16[128,2048]{1,0:T(8,128)(2,1)} %param.17) | copy-start | bytes 1572868
  1.5 10.0 %collective-permute-start = (bf16[2,512]{1,0:T(2,128)(2,1)S(1)}, bf16[2,512]{1,0:T(2,128)(2,1)S(1)}, u32[]{:S(2)}, u32[]{:S(2)}) collective-permute-start(bf16[2,512]{1,0:T(2,128)(2,1)S(1)} %pad_maximum_fusion.1), channel_id=1, source_target_pairs={{0,4},{4,8},{8,12},{1,5},{5,9},{9,13},{2,6},{6,10},{10,14},{3,7},{... | collective-permute-start | bytes 6152 | tf_op jit(solution)/shard_map/ppermute | solution.py:13
  13.5 9.4 %all-to-all-start = ((bf16[4,128,256]{2,1,0:T(8,128)(2,1)}), bf16[4,128,256]{2,1,0:T(8,128)(2,1)S(1)}, u32[]{:S(2)}, u32[]{:S(2)}) async-start(bf16[4,128,256]{2,1,0:T(8,128)(2,1)} %bitcast.3), calls=%async_computation | async-start | bytes 524288 | tf_op jit(solution)/shard_map/all_to_all | solution.py:38
  23.0 3.0 %copy-start.2 = (f32[2048]{0:T(1024)S(1)}, f32[2048]{0:T(1024)}, u32[]{:S(2)}) copy-start(f32[2048]{0:T(1024)} %param.18) | copy-start | bytes 24580
  26.1 20.0 %copy-start.4 = (bf16[2,2048,256]{2,1,0:T(8,128)(2,1)S(1)}, bf16[2,2048,256]{2,1,0:T(8,128)(2,1)}, u32[]{:S(2)}) copy-start(bf16[2,2048,256]{2,1,0:T(8,128)(2,1)} %param.21) | copy-start | bytes 6291460
  45.3 1.7 %copy-start.5 = (bf16[2,2048,256]{2,1,0:T(8,128)(2,1)S(1)}, bf16[2,2048,256]{2,1,0:T(8,128)(2,1)}, u32[]{:S(2)}) copy-start(bf16[2,2048,256]{2,1,0:T(8,128)(2,1)} %param.22) | copy-start | bytes 6291460
  45.3 13.2 %collective-permute-start.3 = (bf16[128,2176]{1,0:T(8,128)(2,1)S(1)}, bf16[128,2176]{1,0:T(8,128)(2,1)S(1)}, u32[]{:S(2)}, u32[]{:S(2)}) collective-permute-start(bf16[128,2176]{1,0:T(8,128)(2,1)S(1)} %bitcast.87), channel_id=1, source_target_pairs={{0,2},{1,3},{2,0},{3,1},{4,6},{5,7},{6,4},{7,5},{8,10},{9,11},{10,... | collective-permute-start | bytes 1671176 | tf_op jit(solution)/shard_map/ppermute | solution.py:17
  46.1 2.0 %collective-permute-start.1 = (bf16[128,2176]{1,0:T(8,128)(2,1)S(1)}, bf16[128,2176]{1,0:T(8,128)(2,1)S(1)}, u32[]{:S(2)}, u32[]{:S(2)}) collective-permute-start(bf16[128,2176]{1,0:T(8,128)(2,1)S(1)} %bitcast.88), channel_id=1, source_target_pairs={{0,1},{1,0},{2,3},{3,2},{4,5},{5,4},{6,7},{7,6},{8,9},{9,8},{10,11... | collective-permute-start | bytes 1671176 | tf_op jit(solution)/shard_map/ppermute | solution.py:17
  58.4 2.0 %collective-permute-start.4 = (bf16[128,2176]{1,0:T(8,128)(2,1)S(1)}, bf16[128,2176]{1,0:T(8,128)(2,1)S(1)}, u32[]{:S(2)}, u32[]{:S(2)}) collective-permute-start(bf16[128,2176]{1,0:T(8,128)(2,1)S(1)} %collective-permute-done.3), channel_id=1, source_target_pairs={{0,1},{1,0},{2,3},{3,2},{4,5},{5,4},{6,7},{7,6},{8,9},{9,8},{10,11... | collective-permute-start | bytes 1671176 | tf_op jit(solution)/shard_map/ppermute | solution.py:17
  58.6 8.3 %collective-permute-start.2 = (bf16[128,2048]{1,0:T(8,128)(2,1)S(1)}, bf16[128,2048]{1,0:T(8,128)(2,1)S(1)}, u32[]{:S(2)}, u32[]{:S(2)}) collective-permute-start(bf16[128,2048]{1,0:T(8,128)(2,1)S(1)} %convolution_convert_fusion.2), channel_id=1, source_target_pairs={{0,1},{1,0},{2,3},{3,2},{4,5},{5,4},{6,7},{7,6},{8,9},{9,8},{10,11... | collective-permute-start | bytes 1572872 | tf_op jit(solution)/shard_map/ppermute | solution.py:17
  62.4 2.0 %collective-permute-start.5 = (bf16[128,2048]{1,0:T(8,128)(2,1)S(1)}, bf16[128,2048]{1,0:T(8,128)(2,1)S(1)}, u32[]{:S(2)}, u32[]{:S(2)}) collective-permute-start(bf16[128,2048]{1,0:T(8,128)(2,1)S(1)} %convolution_convert_fusion.1), channel_id=1, source_target_pairs={{0,1},{1,0},{2,3},{3,2},{4,5},{5,4},{6,7},{7,6},{8,9},{9,8},{10,11... | collective-permute-start | bytes 1572872 | tf_op jit(solution)/shard_map/ppermute | solution.py:17
  64.8 14.0 %collective-permute-start.6 = (bf16[128,2048]{1,0:T(8,128)(2,1)S(1)}, bf16[128,2048]{1,0:T(8,128)(2,1)S(1)}, u32[]{:S(2)}, u32[]{:S(2)}) collective-permute-start(bf16[128,2048]{1,0:T(8,128)(2,1)S(1)} %add_convert_fusion.1), channel_id=1, source_target_pairs={{0,2},{1,3},{2,0},{3,1},{4,6},{5,7},{6,4},{7,5},{8,10},{9,11},{10,... | collective-permute-start | bytes 1572872 | tf_op jit(solution)/shard_map/ppermute | solution.py:17
where the time goes:
time: 97.7 us; the launch traced here: 97.2 us
  blocking collectives  35.7 us (37%)
  waiting for transfers between devices  28.6 us (29%)
  matrix products  11.4 us (12%)
  starting transfers between devices  11.3 us (12%)
  other arithmetic  7.07 us (7%)
  local copies, waits for them, and re-layouts  2.75 us (3%)
    ppermute x6, waiting for transfers between devices, flipped(): lax.ppermute(block, axis, [(i, i ^ bit) for i in range(lax.axis_size(axis...  22.7 us
    all_to_all x1, blocking collectives, route_by_group(): lax.all_to_all(outgoing, 'sp', split_axis=0, concat_axis=0, tiled=True)  18.7 us
    all_to_all x1, blocking collectives, route_by_group(): lax.all_to_all(summed, 'sp', split_axis=0, concat_axis=0, tiled=True)  17 us
    all_to_all x1, waiting for transfers between devices, project(): lax.all_to_all(mixed, 'tp', split_axis=0, concat_axis=1, tiled=True)  5.94 us
    ppermute x1, starting transfers between devices, shifted(): return lax.ppermute(block, axis, route)  4.96 us
    all_to_all x1, starting transfers between devices, project(): lax.all_to_all(mixed, 'tp', split_axis=0, concat_axis=1, tiled=True)  3.41 us
    dot_general x1, matrix products, project(): jnp.dot(token_rows, out_proj, preferred_element_type=jnp.float32)  3.01 us
    ppermute x6, starting transfers between devices, flipped(): lax.ppermute(block, axis, [(i, i ^ bit) for i in range(lax.axis_size(axis...  2.97 us
  transfers between devices with their start and end apart: 8, of which 6 were waited for; matrix products, arithmetic and copies ran while one was open for 13% of the time, Pallas kernels for 0%

commit v1 on v0

--- a/solution.py
+++ b/solution.py
@@ -62,7 +62,21 @@
     rows = jnp.concatenate([normed, labels], axis=1)
     outgoing = jnp.dot(select, rows, preferred_element_type=jnp.float32).astype(jnp.bfloat16)
     outgoing = outgoing.reshape(seq_ranks, capacity, width + LANES)
-    arrived = lax.all_to_all(outgoing, "sp", split_axis=0, concat_axis=0, tiled=True)
+    a_now = lax.psum(1, axis_name="sp")
+    current_block, p_next = (a_now, lax.axis_index("sp"))
+    known = outgoing.shape[0] // current_block
+    small = list(outgoing.shape)
+    small[0] = known
+    x_next = small[0]
+    small[0] = x_next * current_block
+    arrived = jnp.zeros(small, outgoing.dtype)
+    for t in [*range(current_block)]:
+        clean = lax.dynamic_slice_in_dim(outgoing, (p_next ^ t) * known, known, axis=0)
+        if t:
+            clean = lax.ppermute(
+                clean, axis_name="sp", perm=[(i0, i0 ^ t) for i0 in range(current_block)]
+            )
+        arrived = lax.dynamic_update_slice_in_dim(arrived, clean, (p_next ^ t) * x_next, axis=0)
     blocks = {0: arrived.reshape(block_rows, width + LANES)}
     bits = [1 << b for b in range(shards.bit_length() - 1)]
     for bit in reversed(bits):

time: 97.7 us -> 95.6 us (0.979)
  blocking collectives: 35.7 us -> 16.9 us
  waiting for transfers between devices: 28.6 us -> 42 us
  starting transfers between devices: 11.3 us -> 14.3 us
    all_to_all x1 -> x0, blocking collectives: 18.7 us -> none  [route_by_group(): lax.all_to_all(outgoing, 'sp', split_axis=0, concat_axis=0, tiled=True)]
    ppermute x0 -> x3, waiting for transfers between devices: none -> 11.4 us  [route_by_group(): lax.ppermute(clean, axis_name='sp', perm=[(i0, i0 ^ t) for i0 in range(cu...]
    ppermute x0 -> x3, starting transfers between devices: none -> 4.12 us  [route_by_group(): lax.ppermute(clean, axis_name='sp', perm=[(i0, i0 ^ t) for i0 in range(cu...]
    ppermute x6, waiting for transfers between devices: 22.7 us -> 24.7 us  [flipped(): lax.ppermute(block, axis, [(i, i ^ bit) for i in range(lax.axis_size(axis...]
    ppermute x6, starting transfers between devices: 2.97 us -> 1.79 us  [flipped(): lax.ppermute(block, axis, [(i, i ^ bit) for i in range(lax.axis_size(axis...]
  transfers between devices with their start and end apart: 8 -> 11, of which waited for: 6 -> 8; matrix products, arithmetic and copies ran while one was open for 13% -> 13% of each run, Pallas kernels for 0% -> 0%
where the time goes in v1:
time: 95.6 us; the launch traced here: 95.1 us
  waiting for transfers between devices  42 us (44%)
  blocking collectives  16.9 us (18%)
  starting transfers between devices  14.3 us (15%)
  matrix products  11.4 us (12%)
  other arithmetic  7.08 us (7%)
  local copies, waits for them, and re-layouts  3.01 us (3%)
    ppermute x6, waiting for transfers between devices, flipped(): lax.ppermute(block, axis, [(i, i ^ bit) for i in range(lax.axis_size(axis...  24.7 us
    all_to_all x1, blocking collectives, route_by_group(): lax.all_to_all(summed, 'sp', split_axis=0, concat_axis=0, tiled=True)  16.9 us
    ppermute x3, waiting for transfers between devices, route_by_group(): lax.ppermute(clean, axis_name='sp', perm=[(i0, i0 ^ t) for i0 in range(cu...  11.4 us
    all_to_all x1, waiting for transfers between devices, project(): lax.all_to_all(mixed, 'tp', split_axis=0, concat_axis=1, tiled=True)  5.94 us
    ppermute x1, starting transfers between devices, shifted(): return lax.ppermute(block, axis, route)  4.96 us
    ppermute x3, starting transfers between devices, route_by_group(): lax.ppermute(clean, axis_name='sp', perm=[(i0, i0 ^ t) for i0 in range(cu...  4.12 us
    all_to_all x1, starting transfers between devices, project(): lax.all_to_all(mixed, 'tp', split_axis=0, concat_axis=1, tiled=True)  3.41 us
    dot_general x1, matrix products, project(): jnp.dot(token_rows, out_proj, preferred_element_type=jnp.float32)  3.01 us
  transfers between devices with their start and end apart: 11, of which 8 were waited for; matrix products, arithmetic and copies ran while one was open for 13% of the time, Pallas kernels for 0%

profile of v1, /device:TPU:0, one launch (start us, length us, event | category | flops | bytes accessed | tf_op | source)
XLA Modules:
  0.0 95.1 jit_solution(12640609238236185002)
XLA Ops:
  0.0 0.8 slice.127
  0.8 0.7 slice.128
  1.5 5.0 %collective-permute-start = (bf16[2,512]{1,0:T(2,128)(2,1)S(1)}, bf16[2,512]{1,0:T(2,128)(2,1)S(1)}, u32[]{:S(2)}, u32[]{:S(2)}) collective-permute-start(bf16[2,512]{1,0:T(2,128)(2,1)S(1)} %pad_maximum_fusion.1), channel_id=1, source_target_pairs={{0,4},{4,8},{8,12},{1,5},{5,9},{9,13},{2,6},{6,10},{10,14},{3,7},{... | collective-permute-start | bytes 6152 | tf_op jit(solution)/shard_map/ppermute | solution.py:13
  6.5 0.7 fusion.109
  7.2 0.7 and_select_fusion.2
  7.9 0.7 and_select_fusion
  8.6 1.1 %convert_multiply_fusion = f32[512,256]{1,0:T(8,128)S(1)} fusion(bf16[512,256]{1,0:T(8,128)(2,1)} %param.12, bf16[512,256]{1,0:T(8,128)(2,1)} %param.13), kind=kLoop, calls=%fused_computation.74 | loop fusion | flops 393216 | bytes 1048576 | tf_op jit(solution)/shard_map/mul | solution.py:29
  9.7 0.7 fusion.106
  10.6 0.9 fusion.117
  11.6 1.9 %fusion.60 = bf16[512,256]{1,0:T(8,128)(2,1)} fusion(f32[2,256]{1,0:T(2,128)S(1)} %convert_multiply_fusion.1, f32[512,256]{1,0:T(8,128)S(1)} %convert_multiply_fusion, bf16[512,256]{1,0:T(8,128)(2,1)} %param.14, f32[256]{0:T(256)S(1)} %bitcast.100, f32[256]{0:T(256)S(1)} %bitcast.99, f32[256]{0:T(256)S(1)} %bitcast.98), kind=kLoop, calls=%fused_computation.71 | loop fusion | flops 1310720 | bytes 1053696 | tf_op jit(solution)/shard_map/convert_element_type | solution.py:34
  13.5 3.4 %all-to-all-start = ((bf16[4,128,256]{2,1,0:T(8,128)(2,1)}), bf16[4,128,256]{2,1,0:T(8,128)(2,1)S(1)}, u32[]{:S(2)}, u32[]{:S(2)}) async-start(bf16[4,128,256]{2,1,0:T(8,128)(2,1)} %bitcast.3), calls=%async_computation | async-start | bytes 524288 | tf_op jit(solution)/shard_map/all_to_all | solution.py:38
  16.9 5.9 %all-to-all-done = bf16[4,128,256]{2,1,0:T(8,128)(2,1)S(1)} async-done(((bf16[4,128,256]{2,1,0:T(8,128)(2,1)}), bf16[4,128,256]{2,1,0:T(8,128)(2,1)S(1)}, u32[]{:S(2)}, u32[]{:S(2)}) %all-to-all-start) | async-done | bytes 262176 | tf_op jit(solution)/shard_map/all_to_all | solution.py:38
  23.1 3.0 %multiply_reduce_fusion = (f32[128]{0:T(128)S(1)}, f32[128,2048]{1,0:T(8,128)S(1)}) fusion(bf16[128,1024]{0,1:T(8,128)(2,1)S(1)} %bitcast.88, bf16[1024,2048]{1,0:T(8,128)(2,1)} %param.16, bf16[128,2048]{1,0:T(8,128)(2,1)S(1)} %copy-done.1), kind=kOutput, calls=%fused_computation.43 | convolution fusion | flops 537919360 | bytes 6029824 | tf_op jit(solution)/shard_map/dot_general | solution.py:39
  26.7 1.6 %collective-permute-start.1 = (bf16[1,32,2176]{2,1,0:T(8,128)(2,1)S(1)}, bf16[1,32,2176]{2,1,0:T(8,128)(2,1)S(1)}, u32[]{:S(2)}, u32[]{:S(2)}) collective-permute-start(bf16[1,32,2176]{2,1,0:T(8,128)(2,1)S(1)} %get-tuple-element.15), channel_id=1, source_target_pairs={{0,4},{4,0},{8,12},{12,8},{1,5},{5,1},{9,13},{13,9},{2,6},{6,2},{1... | collective-permute-start | bytes 417800 | tf_op jit(solution)/shard_map/ppermute | solution.py:76
  28.3 2.5 %collective-permute-start.3 = (bf16[1,32,2176]{2,1,0:T(8,128)(2,1)S(1)}, bf16[1,32,2176]{2,1,0:T(8,128)(2,1)S(1)}, u32[]{:S(2)}, u32[]{:S(2)}) collective-permute-start(bf16[1,32,2176]{2,1,0:T(8,128)(2,1)S(1)} %get-tuple-element.13), channel_id=1, source_target_pairs={{0,12},{4,8},{8,4},{12,0},{1,13},{5,9},{9,5},{13,1},{2,14},{6,10},... | collective-permute-start | bytes 417800 | tf_op jit(solution)/shard_map/ppermute | solution.py:76
  30.8 1.1 %collective-permute-done.1 = bf16[1,32,2176]{2,1,0:T(8,128)(2,1)S(1)} collective-permute-done((bf16[1,32,2176]{2,1,0:T(8,128)(2,1)S(1)}, bf16[1,32,2176]{2,1,0:T(8,128)(2,1)S(1)}, u32[]{:S(2)}, u32[]{:S(2)}) %collective-permute-start.1) | collective-permute-done | bytes 139296 | tf_op jit(solution)/shard_map/ppermute | solution.py:76
  31.9 10.3 %collective-permute-done.2 = bf16[1,32,2176]{2,1,0:T(8,128)(2,1)S(1)} collective-permute-done((bf16[1,32,2176]{2,1,0:T(8,128)(2,1)S(1)}, bf16[1,32,2176]{2,1,0:T(8,128)(2,1)S(1)}, u32[]{:S(2)}, u32[]{:S(2)}) %collective-permute-start.2) | collective-permute-done | bytes 139296 | tf_op jit(solution)/shard_map/ppermute | solution.py:76
  42.3 0.6 collective-permute-start.6
  43.5 0.3 fusion.32
  44.2 0.7 collective-permute-done.4
  46.4 0.4 convolution_convert_fusion.2
  46.9 9.6 %collective-permute-done.6 = bf16[128,2176]{1,0:T(8,128)(2,1)S(1)} collective-permute-done((bf16[128,2176]{1,0:T(8,128)(2,1)S(1)}, bf16[128,2176]{1,0:T(8,128)(2,1)S(1)}, u32[]{:S(2)}, u32[]{:S(2)}) %collective-permute-start.6) | collective-permute-done | bytes 557088 | tf_op jit(solution)/shard_map/ppermute | solution.py:17
  56.6 0.6 collective-permute-start.5
  57.9 0.5 collective-permute-done.7
  59.9 0.4 convolution_convert_fusion.1
  61.2 1.1 %collective-permute-done.8 = bf16[128,2048]{1,0:T(8,128)(2,1)S(1)} collective-permute-done((bf16[128,2048]{1,0:T(8,128)(2,1)S(1)}, bf16[128,2048]{1,0:T(8,128)(2,1)S(1)}, u32[]{:S(2)}, u32[]{:S(2)}) %collective-permute-start.8) | collective-permute-done | bytes 524320 | tf_op jit(solution)/shard_map/ppermute | solution.py:17
  62.4 0.4 add_convert_fusion.1
  62.8 0.4 collective-permute-start.9
  63.5 0.4 fusion.79
  64.0 12.8 %collective-permute-done.9 = bf16[128,2048]{1,0:T(8,128)(2,1)S(1)} collective-permute-done((bf16[128,2048]{1,0:T(8,128)(2,1)S(1)}, bf16[128,2048]{1,0:T(8,128)(2,1)S(1)}, u32[]{:S(2)}, u32[]{:S(2)}) %collective-permute-start.9) | collective-permute-done | bytes 524320 | tf_op jit(solution)/shard_map/ppermute | solution.py:17
  77.1 16.9 %all_to_all.24 = bf16[4,32,2048]{2,1,0:T(8,128)(2,1)S(1)} all-to-all(bf16[4,32,2048]{2,1,0:T(8,128)(2,1)S(1)} %bitcast.86), channel_id=1, replica_groups=mesh['grp'=2,'sp'=4,'tp'=4] {'sp'}, dimensions={0} | all-to-all | bytes 1048576 | tf_op jit(solution)/shard_map/all_to_all | solution.py:103
  93.9 1.1 %fusion = bf16[128,2048]{1,0:T(8,128)(2,1)} fusion(f32[128,2048]{1,0:T(8,128)S(1)} %get-tuple-element.23, bf16[128,2048]{1,0:T(8,128)(2,1)S(1)} %bitcast.87, s32[128]{0:T(128)S(1)} %multiply_add_fusion), kind=kOutput, calls=%fused_computation.3 | convolution fusion | flops 67649536 | bytes 2097664 | tf_op jit(solution)/shard_map/dot_general | solution.py:104
  (59 shorter events, 7.3 us)
Async XLA Ops:
  0.0 46.4 %copy-start = (bf16[2,256,2048]{2,1,0:T(8,128)(2,1)S(1)}, bf16[2,256,2048]{2,1,0:T(8,128)(2,1)}, u32[]{:S(2)}) copy-start(bf16[2,256,2048]{2,1,0:T(8,128)(2,1)} %param.23) | copy-start | bytes 6291460
  0.0 16.9 %copy-start.3 = (s32[128,2]{0,1:T(2,128)S(1)}, s32[128,2]{0,1:T(2,128)}, u32[]{:S(2)}) copy-start(s32[128,2]{0,1:T(2,128)} %param.19) | copy-start | bytes 3076
  0.0 23.0 %copy-start.1 = (bf16[128,2048]{1,0:T(8,128)(2,1)S(1)}, bf16[128,2048]{1,0:T(8,128)(2,1)}, u32[]{:S(2)}) copy-start(bf16[128,2048]{1,0:T(8,128)(2,1)} %param.17) | copy-start | bytes 1572868
  1.5 10.1 %collective-permute-start = (bf16[2,512]{1,0:T(2,128)(2,1)S(1)}, bf16[2,512]{1,0:T(2,128)(2,1)S(1)}, u32[]{:S(2)}, u32[]{:S(2)}) collective-permute-start(bf16[2,512]{1,0:T(2,128)(2,1)S(1)} %pad_maximum_fusion.1), channel_id=1, source_target_pairs={{0,4},{4,8},{8,12},{1,5},{5,9},{9,13},{2,6},{6,10},{10,14},{3,7},{... | collective-permute-start | bytes 6152 | tf_op jit(solution)/shard_map/ppermute | solution.py:13
  13.5 9.4 %all-to-all-start = ((bf16[4,128,256]{2,1,0:T(8,128)(2,1)}), bf16[4,128,256]{2,1,0:T(8,128)(2,1)S(1)}, u32[]{:S(2)}, u32[]{:S(2)}) async-start(bf16[4,128,256]{2,1,0:T(8,128)(2,1)} %bitcast.3), calls=%async_computation | async-start | bytes 524288 | tf_op jit(solution)/shard_map/all_to_all | solution.py:38
  23.1 3.0 %copy-start.2 = (f32[2048]{0:T(1024)S(1)}, f32[2048]{0:T(1024)}, u32[]{:S(2)}) copy-start(f32[2048]{0:T(1024)} %param.18) | copy-start | bytes 24580
  26.3 16.7 %copy-start.4 = (bf16[2,2048,256]{2,1,0:T(8,128)(2,1)S(1)}, bf16[2,2048,256]{2,1,0:T(8,128)(2,1)}, u32[]{:S(2)}) copy-start(bf16[2,2048,256]{2,1,0:T(8,128)(2,1)} %param.21) | copy-start | bytes 6291460
  26.7 5.2 %collective-permute-start.1 = (bf16[1,32,2176]{2,1,0:T(8,128)(2,1)S(1)}, bf16[1,32,2176]{2,1,0:T(8,128)(2,1)S(1)}, u32[]{:S(2)}, u32[]{:S(2)}) collective-permute-start(bf16[1,32,2176]{2,1,0:T(8,128)(2,1)S(1)} %get-tuple-element.15), channel_id=1, source_target_pairs={{0,4},{4,0},{8,12},{12,8},{1,5},{5,1},{9,13},{13,9},{2,6},{6,2},{1... | collective-permute-start | bytes 417800 | tf_op jit(solution)/shard_map/ppermute | solution.py:76
  28.3 13.9 %collective-permute-start.3 = (bf16[1,32,2176]{2,1,0:T(8,128)(2,1)S(1)}, bf16[1,32,2176]{2,1,0:T(8,128)(2,1)S(1)}, u32[]{:S(2)}, u32[]{:S(2)}) collective-permute-start(bf16[1,32,2176]{2,1,0:T(8,128)(2,1)S(1)} %get-tuple-element.13), channel_id=1, source_target_pairs={{0,12},{4,8},{8,4},{12,0},{1,13},{5,9},{9,5},{13,1},{2,14},{6,10},... | collective-permute-start | bytes 417800 | tf_op jit(solution)/shard_map/ppermute | solution.py:76
  30.8 11.4 %collective-permute-start.2 = (bf16[1,32,2176]{2,1,0:T(8,128)(2,1)S(1)}, bf16[1,32,2176]{2,1,0:T(8,128)(2,1)S(1)}, u32[]{:S(2)}, u32[]{:S(2)}) collective-permute-start(bf16[1,32,2176]{2,1,0:T(8,128)(2,1)S(1)} %get-tuple-element.14), channel_id=1, source_target_pairs={{0,8},{4,12},{8,0},{12,4},{1,9},{5,13},{9,1},{13,5},{2,10},{6,14},... | collective-permute-start | bytes 417800 | tf_op jit(solution)/shard_map/ppermute | solution.py:76
  42.3 1.6 %copy-start.5 = (bf16[2,2048,256]{2,1,0:T(8,128)(2,1)S(1)}, bf16[2,2048,256]{2,1,0:T(8,128)(2,1)}, u32[]{:S(2)}) copy-start(bf16[2,2048,256]{2,1,0:T(8,128)(2,1)} %param.22) | copy-start | bytes 6291460
  42.3 14.1 %collective-permute-start.6 = (bf16[128,2176]{1,0:T(8,128)(2,1)S(1)}, bf16[128,2176]{1,0:T(8,128)(2,1)S(1)}, u32[]{:S(2)}, u32[]{:S(2)}) collective-permute-start(bf16[128,2176]{1,0:T(8,128)(2,1)S(1)} %bitcast.91), channel_id=1, source_target_pairs={{0,2},{1,3},{2,0},{3,1},{4,6},{5,7},{6,4},{7,5},{8,10},{9,11},{10,... | collective-permute-start | bytes 1671176 | tf_op jit(solution)/shard_map/ppermute | solution.py:17
  42.9 2.0 %collective-permute-start.4 = (bf16[128,2176]{1,0:T(8,128)(2,1)S(1)}, bf16[128,2176]{1,0:T(8,128)(2,1)S(1)}, u32[]{:S(2)}, u32[]{:S(2)}) collective-permute-start(bf16[128,2176]{1,0:T(8,128)(2,1)S(1)} %bitcast.92), channel_id=1, source_target_pairs={{0,1},{1,0},{2,3},{3,2},{4,5},{5,4},{6,7},{7,6},{8,9},{9,8},{10,11... | collective-permute-start | bytes 1671176 | tf_op jit(solution)/shard_map/ppermute | solution.py:17
  56.4 2.0 %collective-permute-start.7 = (bf16[128,2176]{1,0:T(8,128)(2,1)S(1)}, bf16[128,2176]{1,0:T(8,128)(2,1)S(1)}, u32[]{:S(2)}, u32[]{:S(2)}) collective-permute-start(bf16[128,2176]{1,0:T(8,128)(2,1)S(1)} %collective-permute-done.6), channel_id=1, source_target_pairs={{0,1},{1,0},{2,3},{3,2},{4,5},{5,4},{6,7},{7,6},{8,9},{9,8},{10,11... | collective-permute-start | bytes 1671176 | tf_op jit(solution)/shard_map/ppermute | solution.py:17
  56.6 7.3 %collective-permute-start.5 = (bf16[128,2048]{1,0:T(8,128)(2,1)S(1)}, bf16[128,2048]{1,0:T(8,128)(2,1)S(1)}, u32[]{:S(2)}, u32[]{:S(2)}) collective-permute-start(bf16[128,2048]{1,0:T(8,128)(2,1)S(1)} %convolution_convert_fusion.2), channel_id=1, source_target_pairs={{0,1},{1,0},{2,3},{3,2},{4,5},{5,4},{6,7},{7,6},{8,9},{9,8},{10,11... | collective-permute-start | bytes 1572872 | tf_op jit(solution)/shard_map/ppermute | solution.py:17
  60.4 2.0 %collective-permute-start.8 = (bf16[128,2048]{1,0:T(8,128)(2,1)S(1)}, bf16[128,2048]{1,0:T(8,128)(2,1)S(1)}, u32[]{:S(2)}, u32[]{:S(2)}) collective-permute-start(bf16[128,2048]{1,0:T(8,128)(2,1)S(1)} %convolution_convert_fusion.1), channel_id=1, source_target_pairs={{0,1},{1,0},{2,3},{3,2},{4,5},{5,4},{6,7},{7,6},{8,9},{9,8},{10,11... | collective-permute-start | bytes 1572872 | tf_op jit(solution)/shard_map/ppermute | solution.py:17
  62.8 14.0 %collective-permute-start.9 = (bf16[128,2048]{1,0:T(8,128)(2,1)S(1)}, bf16[128,2048]{1,0:T(8,128)(2,1)S(1)}, u32[]{:S(2)}, u32[]{:S(2)}) collective-permute-start(bf16[128,2048]{1,0:T(8,128)(2,1)S(1)} %add_convert_fusion.1), channel_id=1, source_target_pairs={{0,2},{1,3},{2,0},{3,1},{4,6},{5,7},{6,4},{7,5},{8,10},{9,11},{10,... | collective-permute-start | bytes 1572872 | tf_op jit(solution)/shard_map/ppermute | solution.py:17
